TPU v7x, 512 devices: a whole 4x4x16 slice. The times are simulated.
512 devices in a mesh: fs: 32 (over z, core), tp: 16 (over y, x).
Axes of the slice: x: 4, y: 4, z: 16, core: 2. Of those that a mesh axis runs over, the one named last changes fastest.
Arguments:
- normed_in: bfloat16 [32768, 2048], P('fs'), may hold values from -6 to 6
- grad_x: bfloat16 [32768, 2048], P('fs', 'tp'), may hold values from -0.044194174 to 0.044194174
- grad_y: bfloat16 [32768, 2048], P('fs', 'tp'), may hold values from -0.044194174 to 0.044194174
- weight_x: float32 [2048, 2048], P('fs', 'tp'), may hold values from -0.125 to 0.125
- weight_y: float32 [2048, 2048], P('fs', 'tp'), may hold values from -0.125 to 0.125
- factor_x: bfloat16 [2048, 512], P('fs'), may hold values from -0.13258252 to 0.13258252
- factor_y: bfloat16 [2048, 512], P('fs'), may hold values from -0.13258252 to 0.13258252
- first_x: float32 [512, 2048], P('fs', 'tp'), may hold values from -8 to 8
- first_y: float32 [512, 2048], P('fs', 'tp'), may hold values from -8 to 8
- second_x: float32 [512, 2048], P('fs', 'tp'), may hold values from 0.5 to 2
- second_y: float32 [512, 2048], P('fs', 'tp'), may hold values from 0.5 to 2
Outputs:
- new_weight_x: float32 [2048, 2048], P('fs', 'tp')
- new_weight_y: float32 [2048, 2048], P('fs', 'tp')
- step_x: float32 [2048, 2048], P('fs', 'tp')
- step_y: float32 [2048, 2048], P('fs', 'tp')
- new_first_x: float32 [512, 2048], P('fs', 'tp')
- new_first_y: float32 [512, 2048], P('fs', 'tp')
- new_second_x: float32 [512, 2048], P('fs', 'tp')
- new_second_y: float32 [512, 2048], P('fs', 'tp')
- copy_x: bfloat16 [2048, 2048], P(None, 'tp')
- copy_y: bfloat16 [2048, 2048], P(None, 'tp')
All inputs are finite; a program needn't handle non-finite values.
Results may differ from a plain program's by a relative error of at most 0.02.
Values may be sent and summed in bfloat16 or wider, within the bound.
A program may use at most 128 MiB of HBM per device.

v0:
```python
import functools

import jax
import jax.numpy as jnp
from jax import lax
from jax.sharding import Mesh
from jax.sharding import PartitionSpec as P

D = 2048
RW = 2048
FS = ("fs_0", "fs_1")
FS_TP = ("fs_0", "fs_1", "tp_0", "tp_1")
TP = ("tp_0", "tp_1")


def sent_together(arrays, axis, dim, along):
    widths = [a.shape[along] for a in arrays]
    both = jnp.concatenate(arrays, axis=along)
    filled = lax.all_gather(both, axis, axis=dim, tiled=True)
    return tuple(jnp.split(filled, [sum(widths[:k]) for k in range(1, len(widths))], axis=along))


def cut_along(x, dim, size):
    before, after = (x.shape[:dim], x.shape[dim + 1 :])
    return jnp.moveaxis(x.reshape(*before, size, -1, *after), dim, 0)


def sent_and_summed(x, axis, dim):
    size = lax.axis_size(axis)
    parts = lax.all_to_all(cut_along(x, dim, size), axis, 0, 0, tiled=True)
    return jnp.sum(parts.astype(jnp.float32), axis=0)


def over_axes(x, axes):
    return functools.reduce(lax.psum, axes, x)


def on_device(
    normed_in,
    grad_x,
    grad_y,
    weight_x,
    weight_y,
    factor_x,
    factor_y,
    first_x,
    first_y,
    second_x,
    second_y,
):
    width = grad_x.shape[1]
    contract = (((0,), (0,)), ((), ()))
    highest = lax.Precision.HIGHEST
    pieces = sent_together((factor_x, factor_y), FS, 0, 1)
    mapped_x = jnp.dot(normed_in, pieces[0], preferred_element_type=jnp.float32)
    mapped_y = jnp.dot(normed_in, pieces[1], preferred_element_type=jnp.float32)
    cotan_x = grad_x.astype(jnp.float32)
    cotan_y = grad_y.astype(jnp.float32)
    low_x = lax.dot_general(mapped_x, cotan_x, contract, precision=highest)
    low_y = lax.dot_general(mapped_y, cotan_y, contract, precision=highest)
    projected = sent_and_summed(jnp.concatenate((low_x, low_y), 1).astype(jnp.bfloat16), FS, 0)
    low_x = projected[:, :width]
    low_y = projected[:, width:]
    new_first_x = 0.8 * first_x + 0.2 * low_x
    new_first_y = 0.8 * first_y + 0.2 * low_y
    new_second_x = 0.9 * second_x + 0.1 * low_x * low_x
    new_second_y = 0.9 * second_y + 0.1 * low_y * low_y
    direction = jnp.concatenate(
        (new_first_x / jnp.sqrt(new_second_x), new_first_y / jnp.sqrt(new_second_y)), 1
    )
    piece = lax.all_gather(direction, FS, axis=0, tiled=True)
    part_x = factor_x.astype(jnp.float32)
    part_y = factor_y.astype(jnp.float32)
    update_x = jnp.dot(part_x, piece[:, :width], precision=highest)
    update_y = jnp.dot(part_y, piece[:, width:], precision=highest)
    total = over_axes(jnp.sum(update_x * update_x) + jnp.sum(update_y * update_y), FS_TP)
    scale = jnp.minimum(1.0, 0.25 * jnp.sqrt(2.0 * D * RW) / jnp.sqrt(total))
    step_x = scale * update_x
    step_y = scale * update_y
    new_x = weight_x - 0.02 * step_x
    new_y = weight_y - 0.02 * step_y
    copy_x, copy_y = sent_together(
        (new_x.astype(jnp.bfloat16), new_y.astype(jnp.bfloat16)), FS, 0, 1
    )
    return (
        new_x,
        new_y,
        step_x,
        step_y,
        new_first_x,
        new_first_y,
        new_second_x,
        new_second_y,
        copy_x,
        copy_y,
    )


def solution(mesh):
    split = Mesh(mesh.devices.reshape(16, 2, 4, 4), ("fs_0", "fs_1", "tp_0", "tp_1"))
    in_specs = (
        P(FS, None),
        P(FS, TP),
        P(FS, TP),
        P(FS, TP),
        P(FS, TP),
        P(FS, None),
        P(FS, None),
        P(FS, TP),
        P(FS, TP),
        P(FS, TP),
        P(FS, TP),
    )
    out_specs = (
        P(FS, TP),
        P(FS, TP),
        P(FS, TP),
        P(FS, TP),
        P(FS, TP),
        P(FS, TP),
        P(FS, TP),
        P(FS, TP),
        P(None, TP),
        P(None, TP),
    )
    return jax.shard_map(
        on_device, mesh=split, in_specs=in_specs, out_specs=out_specs, check_vma=False
    )
```

profile of v0, /device:TPU:1, one launch (start us, length us, event | category | flops | bytes accessed | tf_op | source)
XLA Modules:
  0.0 287.9 jit_solution(4614929683648097152)
XLA Ops:
  7.2 0.0 copy-start
  7.2 0.0 all-gather.3.cloned.1.call-start
  7.2 1.6 pad_maximum_fusion.1
  8.8 0.0 all-gather.3.cloned.1.call-update
  8.8 0.0 all-gather.5.cloned.1.call-start
  8.9 80.9 %all-gather.3.cloned.1.call-done = bf16[2048,1024]{1,0:T(8,128)(2,1)} async-done(((bf16[64,1024]{1,0:T(8,128)(2,1)}), bf16[2048,1024]{1,0:T(8,128)(2,1)}) %all-gather.3.cloned.1.call-update) | async-done | bytes 4194320 | tf_op jit(solution)/shard_map/all_gather | solution.py:19
  89.8 5.3 %fusion.2 = f32[512,1024]{1,0:T(8,128)S(1)} fusion(bf16[1024,2048]{1,0:T(8,128)(2,1)} %param.11, bf16[2048,1024]{1,0:T(8,128)(2,1)} %all-gather.3.cloned.1.call-done), kind=kOutput, calls=%fused_computation.2 | convolution fusion | flops 2147483648 | bytes 8388608 | tf_op jit(solution)/shard_map/dot_general | solution.py:55
  95.1 1.1 convolution_convert_fusion.1
  96.2 0.0 copy-start.1
  96.2 2.4 fusion
  98.6 0.0 copy-start.6
  98.7 0.0 copy-start.7
  98.7 0.0 copy-start.8
  98.7 0.0 copy-start.9
  98.7 0.0 copy-start.2
  98.7 0.0 copy-start.3
  98.7 0.0 copy-start.5
  98.7 1.1 convolution_convert_fusion
  99.8 30.2 %all_to_all.5 = bf16[32,16,256]{2,1,0:T(8,128)(2,1)S(1)} all-to-all(bf16[32,16,256]{2,1,0:T(8,128)(2,1)S(1)} %pad_maximum_fusion), channel_id=1, replica_groups=mesh['fs_0'=16,'fs_1'=2,'tp_0'=4,'tp_1'=4] {'fs_0','fs_1'}, dimensions={0} | all-to-all | bytes 524288 | tf_op jit(solution)/shard_map/all_to_all | solution.py:30
  130.1 0.6 rsqrt_multiply_fusion.1
  130.7 28.7 %all_gather.10 = f32[512,256]{1,0:T(8,128)S(1)} all-gather(f32[16,256]{1,0:T(8,128)S(1)} %pad_maximum_fusion.3), channel_id=1, replica_groups=mesh['fs_0'=16,'fs_1'=2,'tp_0'=4,'tp_1'=4] {'fs_0','fs_1'}, dimensions={0}, use_global_device_ids=true | all-gather | bytes 540672 | tf_op jit(solution)/shard_map/all_gather | solution.py:71
  159.4 0.8 multiply_reduce_fusion.1
  160.3 0.8 multiply_reduce_fusion
  162.4 22.2 %psum.28 = f32[]{:T(128)} all-reduce(f32[]{:T(128)S(6)} %add.27), channel_id=1, replica_groups=mesh['fs_0'=16,'fs_1'=2,'tp_0'=4,'tp_1'=4] {'fs_0'}, use_global_device_ids=true, to_apply=%region_3.0 | all-reduce | flops 1 | bytes 8 | tf_op jit(solution)/shard_map/psum | solution.py:35
  184.7 10.1 %psum.29 = f32[]{:T(128)} all-reduce(f32[]{:T(128)} %psum.28), channel_id=1, replica_groups=mesh['fs_0'=16,'fs_1'=2,'tp_0'=4,'tp_1'=4] {'fs_1'}, use_global_device_ids=true, to_apply=%region_4.0 | all-reduce | flops 1 | bytes 8 | tf_op jit(solution)/shard_map/psum | solution.py:35
  194.8 9.1 %psum.30 = f32[]{:T(128)} all-reduce(f32[]{:T(128)} %psum.29), channel_id=1, replica_groups=mesh['fs_0'=16,'fs_1'=2,'tp_0'=4,'tp_1'=4] {'tp_0'}, use_global_device_ids=true, to_apply=%region_5.0 | all-reduce | flops 1 | bytes 8 | tf_op jit(solution)/shard_map/psum | solution.py:35
  203.8 9.0 %psum.31 = f32[]{:T(128)} all-reduce(f32[]{:T(128)} %psum.30), channel_id=1, replica_groups=mesh['fs_0'=16,'fs_1'=2,'tp_0'=4,'tp_1'=4] {'tp_1'}, use_global_device_ids=true, to_apply=%region_6.0 | all-reduce | flops 1 | bytes 8 | tf_op jit(solution)/shard_map/psum | solution.py:35
  213.6 0.7 fusion.10
  214.2 0.6 pad_maximum_fusion.2
  214.9 0.0 all-gather.5.cloned.1.call-update
  214.9 63.9 %all-gather.5.cloned.1.call-done = bf16[2048,256]{1,0:T(8,128)(2,1)} async-done(((bf16[64,256]{1,0:T(8,128)(2,1)}), bf16[2048,256]{1,0:T(8,128)(2,1)}) %all-gather.5.cloned.1.call-update) | async-done | bytes 1048592 | tf_op jit(solution)/shard_map/all_gather | solution.py:19
  278.8 2.2 fusion.14
  (18 shorter events, 0.1 us)
Async XLA Ops:
  7.2 88.0 %copy-start = (bf16[1024,128]{1,0:T(8,128)(2,1)S(1)}, bf16[1024,128]{1,0:T(8,128)(2,1)}, u32[]{:S(2)}) copy-start(bf16[1024,128]{1,0:T(8,128)(2,1)} %param.12) | copy-start | bytes 786436
  7.2 82.6 %all-gather.3.cloned.1.call-start = ((), (), s32[]{:S(2)}) async-start(), calls=%async_computation.1 | async-start | bytes 4325376 | tf_op jit(solution)/shard_map/all_gather | solution.py:19
  8.8 270.0 %all-gather.5.cloned.1.call-start = ((), (), s32[]{:S(2)}) async-start(), calls=%async_computation.2 | async-start | bytes 1081344 | tf_op jit(solution)/shard_map/all_gather | solution.py:19
  89.8 6.4 %copy-start.10 = (bf16[1024,2048]{1,0:T(8,128)(2,1)S(1)}, bf16[1024,2048]{1,0:T(8,128)(2,1)}, u32[]{:S(2)}) copy-start(bf16[1024,2048]{1,0:T(8,128)(2,1)} %param.11) | copy-start | bytes 12582916
  89.8 6.4 %copy-start.11 = (bf16[2048,1024]{1,0:T(8,128)(2,1)S(1)}, bf16[2048,1024]{1,0:T(8,128)(2,1)}, u32[]{:S(2)}) copy-start(bf16[2048,1024]{1,0:T(8,128)(2,1)} %all-gather.3.cloned.1.call-done) | copy-start | bytes 12582916
  96.2 2.4 copy-start.1
  98.6 31.4 %copy-start.6 = (f32[16,128]{1,0:T(8,128)S(1)}, f32[16,128]{1,0:T(8,128)}, u32[]{:S(2)}) copy-start(f32[16,128]{1,0:T(8,128)} %param.20) | copy-start | bytes 24580
  98.7 31.4 %copy-start.7 = (f32[16,128]{1,0:T(8,128)S(1)}, f32[16,128]{1,0:T(8,128)}, u32[]{:S(2)}) copy-start(f32[16,128]{1,0:T(8,128)} %param.18) | copy-start | bytes 24580
  98.7 31.4 %copy-start.8 = (f32[16,128]{1,0:T(8,128)S(1)}, f32[16,128]{1,0:T(8,128)}, u32[]{:S(2)}) copy-start(f32[16,128]{1,0:T(8,128)} %param.21) | copy-start | bytes 24580
  98.7 31.4 %copy-start.9 = (f32[16,128]{1,0:T(8,128)S(1)}, f32[16,128]{1,0:T(8,128)}, u32[]{:S(2)}) copy-start(f32[16,128]{1,0:T(8,128)} %param.19) | copy-start | bytes 24580
  98.7 60.7 %copy-start.2 = (bf16[64,512]{1,0:T(8,128)(2,1)S(1)}, bf16[64,512]{1,0:T(8,128)(2,1)}, u32[]{:S(2)}) copy-start(bf16[64,512]{1,0:T(8,128)(2,1)} %param.16) | copy-start | bytes 196612
  98.7 61.6 %copy-start.3 = (bf16[64,512]{1,0:T(8,128)(2,1)S(1)}, bf16[64,512]{1,0:T(8,128)(2,1)}, u32[]{:S(2)}) copy-start(bf16[64,512]{1,0:T(8,128)(2,1)} %param.17) | copy-start | bytes 196612
  98.7 114.9 %copy-start.4 = (f32[64,128]{1,0:T(8,128)S(1)}, f32[64,128]{1,0:T(8,128)}, u32[]{:S(2)}) copy-start(f32[64,128]{1,0:T(8,128)} %param.14) | copy-start | bytes 98308
  98.7 114.9 %copy-start.5 = (f32[64,128]{1,0:T(8,128)S(1)}, f32[64,128]{1,0:T(8,128)}, u32[]{:S(2)}) copy-start(f32[64,128]{1,0:T(8,128)} %param.15) | copy-start | bytes 98308
Sparse Core Ops, SparseCore 0:
  10.7 79.0 all-gather.2
  215.0 63.7 all-gather.4
where the time goes:
time: 288 us
  waiting for transfers between devices  145 us (50%)
  blocking collectives  109 us (38%)
  between operations  16.2 us (6%)
  matrix products  11.5 us (4%)
  other arithmetic  3.55 us (1%)
    all_gather x2, waiting for transfers between devices, sent_together(): filled = lax.all_gather(both, axis, axis=dim, tiled=True)  145 us
    psum x4, blocking collectives, over_axes(): return functools.reduce(lax.psum, axes, x)  50.5 us
    all_to_all x1, blocking collectives, sent_and_summed(): parts = lax.all_to_all(cut_along(x, dim, size), axis, 0, 0, tiled=True)  30.2 us
    all_gather x1, blocking collectives, on_device(): piece = lax.all_gather(direction, FS, axis=0, tiled=True)  28.7 us
  transfers between devices with their start and end apart: 2, of which 2 were waited for; matrix products, arithmetic and copies ran while one was open for 0% of the time, Pallas kernels for 0%

commit v1 on v0

v1 whole, which is shorter than its diff:
```python
import functools

import jax
import jax.numpy as jnp
from jax import lax
from jax.experimental import pallas as pl
from jax.experimental.pallas import tpu as pltpu
from jax.sharding import Mesh
from jax.sharding import PartitionSpec as P

D = 2048
RW = 2048
NZ = 16
FS = ("z", "c")
TP = ("y", "x")
MESH_ID = pl.DeviceIdType.MESH
F32 = jnp.float32
BF16 = jnp.bfloat16


def wait_on(ref, sem):
    pltpu.make_async_copy(ref, ref, sem).wait()


def body(
    n_hbm, gx_hbm, gy_hbm, wx_hbm, wy_hbm, fx_hbm, fy_hbm, ax_hbm, ay_hbm, sx_hbm, sy_hbm,
    nwx, nwy, stx, sty, nfx, nfy, nsx, nsy, cpx, cpy,
    n_v, g_v, f_loc, w_loc, m_loc, f_all, g_f, g_in, g_hl, lo_out, lo_in, d_out, d_all,
    u_f, u_b, u_ob, u_of, w_all, w_tmp, w_oth, s_out, s_all,
    ld, za_s, z_r, zb_s, ip_s, ip_r, pr_s, pr_r, wr_s, wr_r, far_s, lo_r, d_r, s_r,
):
    z, c, y, x = (lax.axis_index(k) for k in ("z", "c", "y", "x"))
    zz = lambda k: lax.rem(z + (k + NZ), NZ)
    other = 1 - c
    partner = (z, other, y, x)

    def send(src, dst, ssem, rsem, dev):
        pltpu.make_async_remote_copy(
            src_ref=src, dst_ref=dst, send_sem=ssem, recv_sem=rsem, device_id=dev, device_id_type=MESH_ID
        ).start()

    barrier = pltpu.get_barrier_semaphore()
    place = c * 16 + y * 4 + x

    def at_place(q):
        return (z, q // 16, lax.rem(q // 4, 4), lax.rem(q, 4))

    @pl.loop(1, 5)
    def _(k):
        for cc in range(2):
            for sign in (1, -1):
                pl.semaphore_signal(
                    barrier, inc=1, device_id=(lax.rem(z + sign * k + NZ, NZ), cc, y, x), device_id_type=MESH_ID
                )

    @pl.loop(1, 32)
    def _(k):
        pl.semaphore_signal(barrier, inc=1, device_id=at_place(lax.rem(place + k, 32)), device_id_type=MESH_ID)

    f_in = [pltpu.make_async_copy(r, f_loc.at[i], ld.at[i]) for i, r in enumerate((fx_hbm, fy_hbm))]
    w_in = [pltpu.make_async_copy(r, w_loc.at[i], ld.at[2 + i]) for i, r in enumerate((wx_hbm, wy_hbm))]
    g_ld = [
        pltpu.make_async_copy(r, g_v.at[:, pl.ds(128 * i, 128)], ld.at[4 + i]) for i, r in enumerate((gx_hbm, gy_hbm))
    ]
    m_in = [
        pltpu.make_async_copy(r, m_loc.at[i], ld.at[6 + i]) for i, r in enumerate((ax_hbm, ay_hbm, sx_hbm, sy_hbm))
    ]
    for cp in f_in + w_in + g_ld:
        cp.start()

    @pl.loop(0, NZ)
    def _(i):
        col = pl.multiple_of(128 * lax.rem(z + i + (NZ - 4), NZ), 128)
        pltpu.make_async_copy(
            n_hbm.at[:, pl.ds(col, 128)], n_v.at[:, pl.ds(pl.multiple_of(128 * i, 128), 128)], ld.at[10]
        ).start()

    for cp in m_in:
        cp.start()
    for cp in f_in + w_in:
        cp.wait()

    f_all[4, pl.ds(pl.multiple_of(64 * c, 64), 64), :] = f_loc[c]
    w_all[4, pl.ds(pl.multiple_of(64 * c, 64), 64), :] = w_loc[c].astype(BF16)
    w_tmp[...] = w_loc[other].astype(BF16)
    pl.semaphore_wait(barrier, 47)

    for br, (a, b) in enumerate(((y, x), (x, y))):
        rg, ch = 2 * a + b // 2, lax.rem(b, 2)
        cols = pl.ds(pl.multiple_of(256 * ch, 256), 256)

        @pl.when(c == a // 2)
        def _():
            for n, k in enumerate((4, -4, 3, -3, 2, -2, 1, -1)):
                send(
                    f_loc.at[br, pl.ds(pl.multiple_of(16 * lax.rem(rg, 4), 16), 16), cols],
                    f_all.at[4 - k, pl.ds(pl.multiple_of(16 * rg, 16), 16), cols],
                    za_s.at[br, n],
                    z_r.at[4 - k],
                    (zz(k), br, y, x),
                )

    mine = pl.ds(pl.multiple_of(64 * c, 64), 64)
    theirs = pl.ds(pl.multiple_of(64 * other, 64), 64)
    send(w_tmp, w_all.at[4, mine, :], pr_s.at[0], pr_r.at[0], partner)
    send(f_loc.at[other], f_all.at[4, mine, :], pr_s.at[1], pr_r.at[1], partner)

    right = (zz(1), c, y, x)
    left = (zz(-1), c, y, x)

    def ring(s):
        if s > 1:
            wait_on(w_all.at[(5 - s) % NZ], wr_r.at[0, s - 2])
        send(w_all.at[(5 - s) % NZ], w_all.at[(4 - s) % NZ], wr_s.at[0, s - 1], wr_r.at[0, s - 1], right)
        if s < 8:
            if s > 1:
                wait_on(w_all.at[3 + s], wr_r.at[1, s - 2])
            send(w_all.at[3 + s], w_all.at[4 + s], wr_s.at[1, s - 1], wr_r.at[1, s - 1], left)

    wait_on(w_all.at[4, theirs, :], pr_r.at[0])
    ring(1)

    for cp in g_ld:
        cp.wait()
    wait_on(n_v, ld.at[10])
    for t in range(4):
        cols = slice(512 * t, 512 * t + 512)
        r = lax.dot_general(g_v[...], n_v[:, cols], (((0,), (0,)), ((), ())), preferred_element_type=F32)
        g_f[0, :, cols] = r[:128]
        g_f[1, :, cols] = r[128:]
    send(g_f.at[other], g_in, pr_s.at[2], pr_r.at[2], partner)

    ra = jnp.where(c == 0, y, x)
    rb = jnp.where(c == 0, x, y)

    def part1(lo, n, b):
        rg, ch = 2 * ra + b // 2, lax.rem(b, 2)
        return f_all.at[
            pl.ds(lo, n), pl.ds(pl.multiple_of(16 * rg, 16), 16), pl.ds(pl.multiple_of(256 * ch, 256), 256)
        ]

    def part2(lo, n, a):
        return f_all.at[pl.ds(lo, n), pl.ds(pl.multiple_of(32 * a, 32), 32), :]

    def dev1(k):
        b = lax.rem(rb + k + 4, 4)
        return b, (z, c, jnp.where(c == 0, y, b), jnp.where(c == 0, b, x))

    def dev2(k):
        a = lax.rem(ra + k + 4, 4)
        return a, (z, c, jnp.where(c == 0, a, y), jnp.where(c == 0, x, a))

    groups = ((0, 4), (5, 4), (9, 7))

    def plane_first(g, ph):
        lo, n = groups[g]
        part, dev, me = ((part1, dev1, rb), (part2, dev2, ra))[ph]
        for i, k in enumerate((1, -1)):
            send(part(lo, n, me), part(lo, n, me), ip_s.at[g, ph, i], ip_r.at[g, ph, i], dev(k)[1])

    def plane_second(g, ph):
        lo, n = groups[g]
        h = (n + 1) // 2
        part, dev = ((part1, dev1), (part2, dev2))[ph]
        lft, rgt = dev(-1), dev(1)
        wait_on(part(lo, n, lft[0]), ip_r.at[g, ph, 0])
        send(part(lo, h, lft[0]), part(lo, h, lft[0]), ip_s.at[g, ph, 2], ip_r.at[g, ph, 2], rgt[1])
        wait_on(part(lo, n, rgt[0]), ip_r.at[g, ph, 1])
        send(
            part(lo + h, n - h, rgt[0]), part(lo + h, n - h, rgt[0]), ip_s.at[g, ph, 3], ip_r.at[g, ph, 3], lft[1]
        )

    def plane_third(g, ph):
        lo, n = groups[g]
        h = (n + 1) // 2
        part, dev = ((part1, dev1), (part2, dev2))[ph]
        far = dev(2)[0]
        wait_on(part(lo, h, far), ip_r.at[g, ph, 2])
        wait_on(part(lo + h, n - h, far), ip_r.at[g, ph, 3])

    def slab(i):
        return part1(i, 1, rb)

    wait_on(slab(0), z_r.at[0])
    for m in (4, 3, 2, 1):
        send(slab(0), slab(NZ - m), zb_s.at[0, m - 1], z_r.at[NZ - m], (zz(m), c, y, x))
    wait_on(slab(8), z_r.at[8])
    for m in (3, 2, 1):
        send(slab(8), slab(8 + m), zb_s.at[1, m - 1], z_r.at[8 + m], (zz(-m), c, y, x))
    for i in (1, 2, 3):
        wait_on(slab(i), z_r.at[i])
    plane_first(0, 0)
    for i in (5, 6, 7):
        wait_on(slab(i), z_r.at[i])
    plane_first(1, 0)
    ring(2)
    wait_on(g_in, pr_r.at[2])
    for t in range(4):
        cols = slice(512 * t, 512 * t + 512)
        g = g_f[c, :, cols] + g_in[:, cols]
        hi = g.astype(BF16)
        g_hl[:128, cols] = hi
        g_hl[128:, cols] = (g - hi.astype(F32)).astype(BF16)

    plane_second(0, 0)
    plane_second(1, 0)
    ring(3)
    plane_third(0, 0)
    plane_first(0, 1)
    plane_third(1, 0)
    plane_first(1, 1)
    for i in range(9, 16):
        wait_on(slab(i), z_r.at[i])
    plane_first(2, 0)
    ring(4)
    plane_second(2, 0)
    plane_second(0, 1)
    plane_second(1, 1)
    plane_third(2, 0)
    plane_first(2, 1)
    ring(5)
    plane_third(0, 1)
    plane_third(1, 1)
    wait_on(f_all.at[4, theirs, :], pr_r.at[1])

    def low_of(lo, n):
        return jnp.dot(
            g_hl[:, 128 * lo : 128 * (lo + n)],
            f_all[lo : lo + n].reshape(128 * n, 512),
            preferred_element_type=F32,
        )

    low = low_of(0, 9)
    plane_second(2, 1)
    plane_third(2, 1)
    low = low + low_of(9, 7)
    low = (low[:128] + low[128:]).T
    lo_out[...] = low.astype(BF16).reshape(32, 16, 128)

    @pl.loop(0, NZ)
    def _(i):
        k = lax.rem(i, 2) * (8 + (i + 1) // 2) + (1 - lax.rem(i, 2)) * (8 - i // 2)
        zt = lax.rem(z + k, NZ)
        for ct in range(2):
            @pl.when((k > 0) & (k < NZ))
            def _():
                send(
                    lo_out.at[2 * zt + ct], lo_in.at[c, z], far_s.at[zt, ct], lo_r.at[c, z], (zt, ct, y, x)
                )

    lo_in[c, z] = lo_out[2 * z + c]
    send(lo_out.at[2 * z + other], lo_in.at[c, z], far_s.at[z, other], lo_r.at[c, z], partner)
    ring(6)
    for cp in m_in:
        cp.wait()

    @pl.loop(0, NZ)
    def _(i):
        for b in range(2):
            @pl.when((i != z) | (b != c))
            def _():
                wait_on(lo_in.at[b, i], lo_r.at[b, i])

    for b, (nf, ns) in enumerate(((nfx, nsx), (nfy, nsy))):
        g = jnp.sum(lo_in[b].astype(F32), axis=0)
        first = 0.8 * m_loc[b] + 0.2 * g
        second = 0.9 * m_loc[2 + b] + 0.1 * g * g
        nf[...] = first
        ns[...] = second
        d_out[b] = (first / jnp.sqrt(second)).astype(BF16)

    def far_sent():
        @pl.loop(0, NZ)
        def _(i):
            for b in range(2):
                @pl.when((i != z) | (b != c))
                def _():
                    wait_on(lo_out.at[0], far_s.at[i, b])

    far_sent()

    row = 2 * z + c

    @pl.loop(0, NZ)
    def _(i):
        k = lax.rem(i, 2) * (8 + (i + 1) // 2) + (1 - lax.rem(i, 2)) * (8 - i // 2)
        zt = lax.rem(z + k, NZ)
        for ct in range(2):
            @pl.when((k > 0) & (k < NZ))
            def _():
                send(d_out.at[ct], d_all.at[row], far_s.at[zt, ct], d_r.at[row], (zt, ct, y, x))

    d_all[row] = d_out[c]
    send(d_out.at[other], d_all.at[row], far_s.at[z, other], d_r.at[row], partner)
    ring(7)
    ring(8)
    wait_on(w_all.at[12], wr_r.at[0, 7])
    wait_on(w_all.at[11], wr_r.at[1, 6])
    send(w_all, w_oth, pr_s.at[3], pr_r.at[3], partner)

    @pl.loop(0, 32)
    def _(i):
        @pl.when(i != row)
        def _():
            wait_on(d_all.at[i], d_r.at[i])

    d = d_all[...].reshape(512, 128)
    squares = jnp.zeros((8, 128), F32)
    for t in range(4):
        u = jnp.dot(f_all[4 * t : 4 * t + 4].reshape(512, 512), d, preferred_element_type=F32)
        squares = squares + jnp.sum((u * u).reshape(64, 8, 128), axis=0)
        u_f[4 * t : 4 * t + 4] = u.reshape(4, 128, 128)
        u_b[4 * t : 4 * t + 4] = u.astype(BF16).reshape(4, 128, 128)
    squares = jnp.sum(squares, axis=0, keepdims=True)
    s_out[0] = squares
    s_all[place] = squares
    far_sent()

    @pl.loop(1, 32)
    def _(k):
        q = lax.rem(place + k, 32)
        send(s_out.at[0], s_all.at[place], far_s.at[q // 2, lax.rem(q, 2)], s_r.at[place], at_place(q))

    send(u_f.at[4, theirs, :], u_of, pr_s.at[4], pr_r.at[4], partner)
    send(u_b, u_ob, pr_s.at[5], pr_r.at[5], partner)

    @pl.loop(0, 32)
    def _(i):
        @pl.when(i != place)
        def _():
            wait_on(s_all.at[i], s_r.at[i])

    wait_on(u_of, pr_r.at[4])
    wait_on(u_ob, pr_r.at[5])
    wait_on(w_oth, pr_r.at[3])
    total = jnp.sum(jnp.sum(s_all[...], axis=0), axis=1, keepdims=True)
    scale = jnp.minimum(1.0, 0.25 * (2.0 * D * RW) ** 0.5 / jnp.sqrt(total))

    def finish(br, u_rows, st, nw, cp, wb, ub):
        step = scale * u_rows
        st[...] = step
        nw[...] = w_loc[br] - 0.02 * step

        @pl.loop(0, NZ)
        def _(i):
            at = pl.multiple_of(128 * lax.rem(z + i + (NZ - 4), NZ), 128)
            cp[pl.ds(at, 128), :] = (wb[i].astype(F32) - 0.02 * (scale * ub[i].astype(F32))).astype(BF16)

    @pl.when(c == 0)
    def _():
        finish(0, u_f[4, :64], stx, nwx, cpx, w_all, u_b)
        finish(1, u_of[...], sty, nwy, cpy, w_oth, u_ob)

    @pl.when(c == 1)
    def _():
        finish(1, u_f[4, 64:], sty, nwy, cpy, w_all, u_b)
        finish(0, u_of[...], stx, nwx, cpx, w_oth, u_ob)

    for br, a in enumerate((y, x)):
        @pl.when(c == a // 2)
        def _():
            for n in range(8):
                wait_on(slab(0), za_s.at[br, n])
    for m in range(4):
        wait_on(slab(0), zb_s.at[0, m])
    for m in range(3):
        wait_on(slab(0), zb_s.at[1, m])
    for g, (lo, n) in enumerate(groups):
        h = (n + 1) // 2
        for ph, (part, me) in enumerate(((part1, rb), (part2, ra))):
            for i, nn in enumerate((n, n, h, n - h)):
                wait_on(part(lo, nn, me), ip_s.at[g, ph, i])
    for i, r in enumerate((w_tmp, f_loc.at[0], g_in, w_oth, u_of, u_ob)):
        wait_on(r, pr_s.at[i])
    for s in range(8):
        wait_on(w_all.at[0], wr_s.at[0, s])
    for s in range(7):
        wait_on(w_all.at[0], wr_s.at[1, s])

    @pl.loop(1, 32)
    def _(k):
        q = lax.rem(place + k, 32)
        wait_on(s_out.at[0], far_s.at[q // 2, lax.rem(q, 2)])


def on_device(*args):
    out = lambda s, t: jax.ShapeDtypeStruct(s, t)
    dma = pltpu.SemaphoreType.DMA
    return pl.pallas_call(
        body,
        out_shape=[out((64, 128), F32)] * 4 + [out((16, 128), F32)] * 4 + [out((D, 128), BF16)] * 2,
        in_specs=[pl.BlockSpec(memory_space=pltpu.HBM)] * 11,
        out_specs=[pl.BlockSpec(memory_space=pltpu.VMEM)] * 10,
        scratch_shapes=[
            pltpu.VMEM((1024, D), BF16),
            pltpu.VMEM((1024, 256), BF16),
            pltpu.VMEM((2, 64, 512), BF16),
            pltpu.VMEM((2, 64, 128), F32),
            pltpu.VMEM((4, 16, 128), F32),
            pltpu.VMEM((NZ, 128, 512), BF16),
            pltpu.VMEM((2, 128, D), F32),
            pltpu.VMEM((128, D), F32),
            pltpu.VMEM((256, D), BF16),
            pltpu.VMEM((32, 16, 128), BF16),
            pltpu.VMEM((2, NZ, 16, 128), BF16),
            pltpu.VMEM((2, 16, 128), BF16),
            pltpu.VMEM((32, 16, 128), BF16),
            pltpu.VMEM((NZ, 128, 128), F32),
            pltpu.VMEM((NZ, 128, 128), BF16),
            pltpu.VMEM((NZ, 128, 128), BF16),
            pltpu.VMEM((64, 128), F32),
            pltpu.VMEM((NZ, 128, 128), BF16),
            pltpu.VMEM((64, 128), BF16),
            pltpu.VMEM((NZ, 128, 128), BF16),
            pltpu.VMEM((1, 1, 128), F32),
            pltpu.VMEM((32, 1, 128), F32),
            dma((11,)),
            dma((2, 8)),
            dma((NZ,)),
            dma((2, 4)),
            dma((3, 2, 4)),
            dma((3, 2, 4)),
            dma((6,)),
            dma((6,)),
            dma((2, 8)),
            dma((2, 8)),
            dma((NZ, 2)),
            dma((2, NZ)),
            dma((32,)),
            dma((32,)),
        ],
        compiler_params=pltpu.CompilerParams(
            collective_id=0, has_side_effects=True, vmem_limit_bytes=48 * 1024 * 1024
        ),
        name="update",
    )(*args)


def solution(mesh):
    split = Mesh(mesh.devices.reshape(NZ, 2, 4, 4), ("z", "c", "y", "x"))
    both = P(FS, TP)
    rows = P(FS, None)
    in_specs = (rows, both, both, both, both, rows, rows, both, both, both, both)
    out_specs = (both,) * 8 + (P(None, TP),) * 2
    return jax.shard_map(on_device, mesh=split, in_specs=in_specs, out_specs=out_specs, check_vma=False)
```

time: 288 us -> 92.4 us (0.32)
  waiting for transfers between devices: 145 us -> 0 us
  blocking collectives: 109 us -> 0 us
  Pallas kernels: 0 us -> 74.7 us
  between operations: 16.2 us -> 0.68 us
  local copies, waits for them, and re-layouts: 2.31 us -> 16.5 us
  matrix products: 11.5 us -> 0 us
  other arithmetic: 3.55 us -> 0 us
    all_gather x2 -> x0, waiting for transfers between devices: 145 us -> none  [sent_together(): filled = lax.all_gather(both, axis, axis=dim, tiled=True)]
    pallas_call x0 -> x1, Pallas kernels: none -> 74.7 us  [on_device(): pl.pallas_call(body, out_shape=[out((64, 128), F32)] * 4 + [out((16, 128)...]
    psum x4 -> x0, blocking collectives: 50.5 us -> none  [over_axes(): return functools.reduce(lax.psum, axes, x)]
    all_to_all x1 -> x0, blocking collectives: 30.2 us -> none  [sent_and_summed(): parts = lax.all_to_all(cut_along(x, dim, size), axis, 0, 0, tiled=True)]
    all_gather x1 -> x0, blocking collectives: 28.7 us -> none  [on_device(): piece = lax.all_gather(direction, FS, axis=0, tiled=True)]
    unnamed x24 -> x32, local copies, waits for them, and re-layouts: 0.07 us -> 16.5 us
    dot_general x6 -> x0, matrix products: 11.5 us -> none  [the longest x1 5.35 us: on_device(): mapped_x = jnp.dot(normed_in, pieces[0], preferred_element_type=jnp.float32)]
  transfers between devices with their start and end apart: 2 -> 0, of which waited for: 2 -> 0; matrix products, arithmetic and copies ran while one was open for 0% -> 0% of each run, Pallas kernels for 0% -> 0%
where the time goes in v1:
time: 92.4 us; the launch traced here: 91.8 us
  Pallas kernels  74.7 us (81%)
  local copies, waits for them, and re-layouts  16.5 us (18%)
    pallas_call x1, Pallas kernels, on_device(): pl.pallas_call(body, out_shape=[out((64, 128), F32)] * 4 + [out((16, 128)...  74.7 us
    unnamed x32, local copies, waits for them, and re-layouts  16.5 us

profile of v1, /device:TPU:1, one launch (start us, length us, event | category | flops | bytes accessed | tf_op | source)
XLA Modules:
  0.0 91.8 jit_solution(16599517327871401749)
XLA Ops:
  0.6 0.0 copy-start
  0.7 2.2 %copy-done = bf16[1024,2048]{1,0:T(8,128)(2,1)S(1)} copy-done((bf16[1024,2048]{1,0:T(8,128)(2,1)S(1)}, bf16[1024,2048]{1,0:T(8,128)(2,1)}, u32[]{:S(2)}) %copy-start) | copy-done | bytes 4194328
  2.8 0.0 copy-start.1
  2.8 0.9 %copy-done.1 = bf16[1024,128]{1,0:T(8,128)(2,1)S(1)} copy-done((bf16[1024,128]{1,0:T(8,128)(2,1)S(1)}, bf16[1024,128]{1,0:T(8,128)(2,1)}, u32[]{:S(2)}) %copy-start.1) | copy-done | bytes 262168
  3.8 0.0 copy-start.2
  3.8 0.9 %copy-done.2 = bf16[1024,128]{1,0:T(8,128)(2,1)S(1)} copy-done((bf16[1024,128]{1,0:T(8,128)(2,1)S(1)}, bf16[1024,128]{1,0:T(8,128)(2,1)}, u32[]{:S(2)}) %copy-start.2) | copy-done | bytes 262168
  4.7 0.0 copy-start.3
  4.7 0.8 copy-done.3
  5.6 0.0 copy-start.4
  5.6 0.8 copy-done.4
  6.4 0.0 copy-start.5
  6.4 0.8 copy-done.5
  7.2 0.0 copy-start.6
  7.2 0.8 copy-done.6
  7.9 0.0 copy-start.7
  7.9 0.7 copy-done.7
  8.6 0.0 copy-start.8
  8.6 0.7 copy-done.8
  9.3 0.0 copy-start.9
  9.3 0.7 copy-done.9
  10.0 0.7 copy-done.10
  10.7 74.7 %update.1 = (f32[64,128]{1,0:T(8,128)S(1)}, f32[64,128]{1,0:T(8,128)S(1)}, f32[64,128]{1,0:T(8,128)S(1)}, f32[64,128]{1,0:T(8,128)S(1)}, f32[16,128]{1,0:T(8,128...) custom-call(bf16[1024,2048]{1,0:T(8,128)(2,1)S(1)} %copy-done, ...), custom_call_target="tpu_custom_call" | custom-call | tf_op jit(solution)/shard_map/update/pallas_call | solution.py:389
  85.4 0.6 copy.31
  86.0 0.6 copy.32
  86.6 0.6 copy.33
  87.2 0.6 copy.34
  87.8 0.6 copy.35
  88.4 0.6 copy.36
  89.0 0.6 copy.37
  89.6 0.6 copy.38
  90.2 0.8 copy.39
  91.0 0.8 copy.40
  (1 shorter events, 0.0 us)
Async XLA Ops:
  0.6 2.2 %copy-start = (bf16[1024,2048]{1,0:T(8,128)(2,1)S(1)}, bf16[1024,2048]{1,0:T(8,128)(2,1)}, u32[]{:S(2)}) copy-start(bf16[1024,2048]{1,0:T(8,128)(2,1)} %n_hbm.1) | copy-start | bytes 12582916
  2.8 0.9 %copy-start.1 = (bf16[1024,128]{1,0:T(8,128)(2,1)S(1)}, bf16[1024,128]{1,0:T(8,128)(2,1)}, u32[]{:S(2)}) copy-start(bf16[1024,128]{1,0:T(8,128)(2,1)} %gx_hbm.1) | copy-start | bytes 786436
  3.8 0.9 %copy-start.2 = (bf16[1024,128]{1,0:T(8,128)(2,1)S(1)}, bf16[1024,128]{1,0:T(8,128)(2,1)}, u32[]{:S(2)}) copy-start(bf16[1024,128]{1,0:T(8,128)(2,1)} %gy_hbm.1) | copy-start | bytes 786436
  4.7 0.8 copy-start.3
  5.6 0.8 copy-start.4
  6.4 0.8 copy-start.5
  7.2 0.8 copy-start.6
  7.9 0.7 copy-start.7
  8.6 0.7 copy-start.8
  9.3 0.7 copy-start.9
  10.0 0.7 copy-start.10
